TPU v7x, 1024 devices: a whole 4x8x16 slice. The times are simulated.
1024 devices in a mesh: sp: 16 (over z), dp: 64 (over y, x, core).
Axes of the slice: x: 4, y: 8, z: 16, core: 2. Of those that a mesh axis runs over, the one named last changes fastest.
Arguments:
- mixing_input: bfloat16 [64, 2048, 2048], P('dp', 'sp'), may hold values from -6 to 6
- cotangent: bfloat16 [64, 2048, 2048], P('dp', 'sp'), may hold values from -6 to 6
- filter_taps: bfloat16 [4, 2048], P(None, 'sp'), may hold values from -3 to 3
- recurrence_gate_map: bfloat16 [2, 16, 128, 128], P(None, 'sp'), may hold values from -0.5 to 0.5
- input_gate_map: bfloat16 [2, 16, 128, 128], P(None, 'sp'), may hold values from -0.5 to 0.5
- decay_logit_param: float32 [2, 2048], P(None, 'sp')
- spike_decay: float32 [64, 16, 2048], P('dp', 'sp'), may hold values from -2 to -4.8828125e-05
Outputs:
- grad_input: bfloat16 [64, 2048, 2048], P('dp', 'sp')
- grad_rate_map: float32 [2, 16, 128, 128], P(None, 'sp')
- grad_input_map: float32 [2, 16, 128, 128], P(None, 'sp')
- grad_conv_taps: float32 [4, 2048], P(None, 'sp')
All inputs are finite; a program needn't handle non-finite values.
Results may differ from a plain program's by a relative error of at most 0.0075.
Values may be sent and summed in bfloat16 or wider, within the bound.
A program may use at most 64 MiB of HBM per device.

v0:
```python
import functools
import math

import jax
import jax.numpy as jnp
from jax import lax
from jax.experimental import pallas as pl
from jax.experimental.pallas import tpu as pltpu
from jax.sharding import PartitionSpec as P

MESH = pl.DeviceIdType.MESH
TB = 128
F32 = jnp.float32
BF16 = jnp.bfloat16
STRENGTH = 8.0


def grid_of(dp):
    return (8, 4, 2) if dp == 64 else (dp // 4, 2, 2)


def log_keep_of(logit):
    u = jnp.exp(-jnp.abs(logit))
    series = u * (1.0 - u * (0.5 - u * (1.0 / 3.0 - u * 0.25)))
    return jnp.minimum(logit, 0.0) - jnp.where(u < 0.01, series, jnp.log(1.0 + u))


def sigmoid(x):
    return 1.0 / (1.0 + jnp.exp(-x))


def one_less_square(log_decay, decay):
    y = -2.0 * log_decay
    series = y * (1.0 - y * (0.5 - y * (1.0 / 6.0 - y * (1.0 / 24.0 - y * (1.0 / 120.0)))))
    return jnp.where(y < 0.125, series, 1.0 - decay * decay)


def shifted(value, step, forward):
    return pltpu.roll(value, step if forward else 8 - step, 1)


def prefixes(coeff, row, forward):
    outs, product = [], coeff
    for step in (1, 2, 4):
        inside = (row >= step) if forward else (row < 8 - step)
        outs.append(jnp.where(inside, product, 0.0))
        product = jnp.where(inside, product * shifted(product, step, forward), product)
    return outs, product


def doubled(value, steps, forward):
    for step, coeff in zip((1, 2, 4), steps):
        value = value + coeff * shifted(value, step, forward)
    return value


def last_row(value, forward):
    edge = value[7:8] if forward else value[0:1]
    return jnp.broadcast_to(edge, value.shape)


def kernel(
    sizes,
    x_hbm,
    cot_hbm,
    taps_hbm,
    wr_hbm,
    wi_hbm,
    logit_hbm,
    spike_hbm,
    gi_ref,
    gr_ref,
    gm_ref,
    gt_ref,
    taps_ref,
    wr_ref,
    wi_ref,
    logit_ref,
    spike_ref,
    xr,
    cr,
    xf,
    vs,
    vt,
    wcat,
    pre,
    af,
    sc,
    e1,
    e2,
    c2,
    c3,
    qs,
    gs,
    ends,
    carries,
    zs,
    vd,
    vg,
    bk,
    go,
    halves,
    core_in,
    x_out,
    x_in,
    y_out,
    y_in,
    g2,
    g1,
    g0,
    local_sem,
    small_sem,
    z_send,
    x_recv,
    c_recv,
    o_recv,
    r_send,
    r_recv,
):
    n, ny, nx, nc, norm = sizes
    length = n * TB
    me = lax.axis_index("sp")
    dp = lax.axis_index("dp")
    core = lax.rem(dp, nc)
    xi = lax.rem(dp // nc, nx)
    yi = dp // (nc * nx)

    def at_plane(y, x, c):
        return {"sp": me, "dp": (y * nx + x) * nc + c}

    def along_z(peer):
        return {"sp": peer, "dp": dp}

    offsets = [n // 2]
    for d in range(n // 2 - 1, 0, -1):
        offsets += [d, n - d]
    x_peers = [lax.rem(xi + d, nx) for d in range(1, nx)]
    y_peers = [lax.rem(yi + d, ny) for d in range(1, ny)]
    partner = at_plane(yi, xi, 1 - core)

    barrier = pltpu.get_barrier_semaphore()
    greet = [along_z(lax.rem(me + d, n)) for d in offsets]
    greet += [at_plane(yi, x, core) for x in x_peers]
    greet += [at_plane(y, xi, core) for y in y_peers]
    greet += [partner]
    for device in greet:
        pl.semaphore_signal(barrier, inc=1, device_id=device, device_id_type=MESH)

    def columns(ref, block):
        return ref.at[0, :, pl.ds(pl.multiple_of(block * TB, TB), TB)]

    def rows_of(ref, block):
        return ref.at[pl.ds(pl.multiple_of(block * TB, TB), TB)]

    own = [
        pltpu.make_async_copy(columns(x_hbm, me), rows_of(xr, me), local_sem.at[0]),
        pltpu.make_async_copy(columns(cot_hbm, me), rows_of(cr, me), local_sem.at[1]),
    ]
    own[0].start()
    own[1].start()
    small = [
        pltpu.make_async_copy(source, target, small_sem.at[j])
        for j, (source, target) in enumerate(
            (
                (taps_hbm, taps_ref),
                (wr_hbm, wr_ref),
                (wi_hbm, wi_ref),
                (logit_hbm, logit_ref),
                (spike_hbm, spike_ref),
            )
        )
    ]
    for copy in small:
        copy.start()
    pl.semaphore_wait(barrier, len(greet))

    def inward(which, k):
        source, target = ((x_hbm, xr), (cot_hbm, cr))[which]
        peer = lax.rem(me + offsets[k], n)
        return pltpu.make_async_remote_copy(
            src_ref=columns(source, peer),
            dst_ref=rows_of(target, me),
            send_sem=z_send,
            recv_sem=x_recv if which == 0 else c_recv.at[k],
            device_id=along_z(peer),
            device_id_type=MESH,
        )

    def cotangent_arrived(k):
        near = n // 2 - (k + 1) // 2
        origin = lax.rem(me + n - ((k % 2) * near + (1 - k % 2) * (n - near)), n)
        pltpu.make_async_copy(rows_of(cr, origin), rows_of(cr, origin), c_recv.at[k]).wait()
        return origin

    def wait_for_blocks(sem, count):
        rows = pl.ds(0, count * TB)
        pltpu.make_async_copy(xr.at[rows], xr.at[rows], sem).wait()

    for which in range(2):
        for k in range(n - 1):
            inward(which, k).start()

    for copy in small:
        copy.wait()
    zero_rows = jnp.zeros((8, TB), F32)
    xf[0:8, :] = zero_rows
    xf[length + 8 : length + 16, :] = zero_rows
    for edge in (0, length + 16):
        vd[edge : edge + 16, :] = jnp.zeros((16, TB), F32)
        bk[edge : edge + 16, :] = jnp.zeros((16, 512), BF16)
    for d in range(2):
        af[d, 0:8, :] = zero_rows
        af[d, length + 8 : length + 16, :] = zero_rows
        wcat[:, 256 * d : 256 * d + 128] = wr_ref[d, 0]
        wcat[:, 256 * d + 128 : 256 * d + 256] = wi_ref[d, 0]
    taps = [taps_ref[k : k + 1, :].astype(F32) for k in range(4)]
    keep = [STRENGTH * log_keep_of(logit_ref[d : d + 1, :]) for d in range(2)]
    row = lax.broadcasted_iota(jnp.int32, (8, 8, TB), 1)
    row0 = lax.broadcasted_iota(jnp.int32, (8, TB), 0)

    own[0].wait()
    wait_for_blocks(x_recv, n - 1)

    @pl.loop(0, n)
    def _(b):
        at = pl.multiple_of(b * TB, TB)
        xf[pl.ds(at + 8, TB), :] = xr[pl.ds(at, TB), :].astype(F32)

    @pl.loop(0, n)
    def _(b):
        at = pl.multiple_of(b * TB, TB)
        v = xf[pl.ds(at + 6, TB), :] * taps[0]
        for k in range(1, 4):
            v = v + xf[pl.ds(at + 6 + k, TB), :] * taps[k]
        low = v.astype(BF16)
        vs[pl.ds(at, TB), :] = low
        vt[:, pl.ds(at, TB)] = jnp.transpose(low.astype(F32)).astype(BF16)

    chunk = min(512, length)

    @pl.loop(0, length // chunk)
    def _(b):
        at = pl.multiple_of(b * chunk, chunk)
        pre[pl.ds(at, chunk), :] = jnp.dot(
            vs[pl.ds(at, chunk), :], wcat[...], preferred_element_type=F32
        )

    @pl.loop(0, n)
    def _(b):
        at = pl.multiple_of(b * TB, TB)
        spike = jnp.transpose(jnp.broadcast_to(spike_ref[pl.ds(b, 1), :], (TB, TB)))
        v = vs[pl.ds(at, TB), :].astype(F32)
        for d in range(2):
            rate = sigmoid(pre[pl.ds(at, TB), 256 * d : 256 * d + 128])
            gate = sigmoid(pre[pl.ds(at, TB), 256 * d + 128 : 256 * d + 256])
            log_decay = rate * keep[d] + spike
            decay = jnp.exp(log_decay)
            square = one_less_square(log_decay, decay)
            inverse = lax.rsqrt(square)
            multiplier = square * inverse
            gated = gate * v
            source = multiplier * gated
            slope = keep[d] * rate * (1.0 - rate)
            sloped = decay * slope
            af[d, pl.ds(at + 8, TB), :] = decay
            sc[d, pl.ds(at, TB), :] = source
            e1[d, pl.ds(at, TB), :] = sloped
            e2[d, pl.ds(at, TB), :] = -gated * decay * sloped * inverse
            c2[d, pl.ds(at, TB), :] = source * (1.0 - gate)
            c3[d, pl.ds(at, TB), :] = multiplier * gate

    def state_pass(d, block, carry):
        forward = d == 0
        at = pl.multiple_of(block * 64, 64)
        coeff = af[d, pl.ds(at + 8, 64), :].reshape(8, 8, TB)
        steps, product = prefixes(coeff, row, forward)
        value = doubled(sc[d, pl.ds(at, 64), :].reshape(8, 8, TB), steps, forward)
        for g in range(8) if forward else range(7, -1, -1):
            state = value[g] + product[g] * carry
            edge = (row0 == 0) if forward else (row0 == 7)
            before = jnp.where(edge, carry, pltpu.roll(state, 1 if forward else 7, 0))
            spot = pl.ds(at + 8 * g, 8)
            e1[d, spot, :] = before * e1[d, spot, :] + e2[d, spot, :]
            carry = last_row(state, forward)
        return carry

    def state_step(i, carry):
        ahead = state_pass(0, i, carry[0])
        back = state_pass(1, length // 64 - 1 - i, carry[1])
        return ahead, back

    start = jnp.zeros((8, TB), F32)
    lax.fori_loop(0, length // 64, state_step, (start, start))

    @pl.loop(0, n)
    def _(b):
        at = pl.multiple_of(b * TB, TB)
        for d in range(2):
            forward = d == 1
            shift = -1 if forward else 1
            carry = jnp.ones((8, TB), F32)
            for part in (0, 1) if forward else (1, 0):
                coeff = af[d, pl.ds(at + 64 * part + 8 + shift, 64), :].reshape(8, 8, TB)
                steps, product = prefixes(coeff, row, forward)
                for j, step in enumerate(steps):
                    qs[d, j, pl.ds(at + 64 * part, 64), :] = step.reshape(64, TB)
                qs[d, 3, pl.ds(at + 64 * part, 64), :] = product.reshape(64, TB)
                for g in range(8) if forward else range(7, -1, -1):
                    whole = product[g] * carry
                    gs[d, pl.ds(at + 64 * part + 8 * g, 8), :] = whole
                    carry = last_row(whole, forward)
            ends[d, 0, pl.ds(pl.multiple_of(b * 8, 8), 8), :] = carry

    def local_scan(d, block):
        forward = d == 1
        at = pl.multiple_of(block * TB, TB)
        carry = None
        for part in (0, 1) if forward else (1, 0):
            spot = pl.ds(at + 64 * part, 64)
            steps = [qs[d, j, spot, :].reshape(8, 8, TB) for j in range(3)]
            value = doubled(cr[spot, :].astype(F32).reshape(8, 8, TB), steps, forward)
            product = qs[d, 3, spot, :].reshape(8, 8, TB)
            for g in range(8) if forward else range(7, -1, -1):
                adjoint = value[g] if carry is None else value[g] + product[g] * carry
                zs[d, pl.ds(at + 64 * part + 8 * g, 8), :] = adjoint
                carry = last_row(adjoint, forward)
        ends[d, 1, pl.ds(pl.multiple_of(block * 8, 8), 8), :] = carry

    own[1].wait()
    local_scan(0, me)
    local_scan(1, me)

    @pl.loop(0, n - 1)
    def _(k):
        origin = cotangent_arrived(k)
        local_scan(0, origin)
        local_scan(1, origin)

    ahead = back = start
    for b in range(n):
        carries[1, 8 * b : 8 * b + 8, :] = ahead
        ahead = ends[1, 1, 8 * b : 8 * b + 8, :] + ends[1, 0, 8 * b : 8 * b + 8, :] * ahead
        r = n - 1 - b
        carries[0, 8 * r : 8 * r + 8, :] = back
        back = ends[0, 1, 8 * r : 8 * r + 8, :] + ends[0, 0, 8 * r : 8 * r + 8, :] * back

    @pl.loop(0, n)
    def _(b):
        incoming = [carries[d, pl.ds(pl.multiple_of(b * 8, 8), 8), :] for d in range(2)]
        for part in range(4):
            at = pl.multiple_of(b * TB + 32 * part, 32)
            spot, padded = pl.ds(at, 32), pl.ds(at + 16, 32)
            total = None
            for d in range(2):
                local = zs[d, spot, :].reshape(4, 8, TB)
                spread = gs[d, spot, :].reshape(4, 8, TB) * incoming[d][None]
                adjoint = (local + spread).reshape(32, TB)
                bk[padded, 256 * d : 256 * d + 128] = (adjoint * e1[d, spot, :]).astype(BF16)
                bk[padded, 256 * d + 128 : 256 * d + 256] = (adjoint * c2[d, spot, :]).astype(BF16)
                piece_of = adjoint * c3[d, spot, :]
                total = piece_of if total is None else total + piece_of
            vd[padded, :] = total

    def outward(block):
        return pltpu.make_async_remote_copy(
            src_ref=rows_of(go, block),
            dst_ref=columns(gi_ref, me),
            send_sem=z_send,
            recv_sem=o_recv,
            device_id=along_z(block),
            device_id_type=MESH,
        )

    group = max(1, n // 4)
    span = group * TB

    def input_grad(step, sums):
        turn = (1 - step // 2) * (2 + step) + (step // 2) * (3 - step)
        part = lax.rem(me // group + turn, n // group)
        base = pl.multiple_of(part * span, span)
        vg[...] = vd[pl.ds(base, span + 32), :] + lax.dot_general(
            bk[pl.ds(base, span + 32), :],
            wcat[...],
            (((1,), (1,)), ((), ())),
            preferred_element_type=F32,
        )
        for inner in range(group):
            block = part * group + inner
            at = pl.multiple_of(block * TB, TB)
            low = 16 + inner * TB
            here = vg[low : low + TB, :]
            total = here * taps[2]
            for j in (0, 1, 3):
                total = total + vg[low + 2 - j : low + 2 - j + TB, :] * taps[j]
            go[pl.ds(at, TB), :] = total.astype(BF16)

            @pl.when(block != me)
            def _(block=block):
                outward(block).start()

            sums = tuple(
                sums[j]
                + jnp.sum((xf[pl.ds(at + 6 + j, TB), :] * here).reshape(TB // 8, 8, TB), axis=0)
                for j in range(4)
            )
        return sums

    sums = lax.fori_loop(0, n // group, input_grad, (start,) * 4)
    own_out = pltpu.make_async_copy(rows_of(go, me), columns(gi_ref, me), local_sem.at[2])
    own_out.start()

    maps = jnp.dot(vt[...], bk[16 : length + 16, :], preferred_element_type=F32)
    half = 512 // nc
    third = half // nx
    piece = third // ny
    tap_rows = [jnp.sum(s, axis=0, keepdims=True) for s in sums]
    tile = jnp.concatenate(tap_rows + [jnp.zeros((4, TB), F32)], axis=0)
    ordered = jnp.concatenate([maps[:, 128 * j : 128 * j + 128] for j in (0, 2, 1, 3)], axis=0)
    for c in range(nc):
        halves[c, 0:half, :] = ordered[half * c : half * (c + 1)]
        halves[c, half : half + 8, :] = tile

    def exchange(source, target, device, k):
        return pltpu.make_async_remote_copy(
            src_ref=source,
            dst_ref=target,
            send_sem=r_send.at[k],
            recv_sem=r_recv.at[k],
            device_id=device,
            device_id_type=MESH,
        )

    sent = []

    def stage(copies):
        for copy in copies:
            copy.start()
        sent.extend(copies)
        for copy in copies:
            copy.wait_recv()

    base = 0
    stage([exchange(halves.at[1 - core], core_in, partner, base)])
    base += 1
    mine = halves[pl.ds(core, 1)][0] + core_in[...]
    for j in range(nx):
        x_out[j, 0:third, :] = mine[third * j : third * (j + 1)]
        x_out[j, third : third + 8, :] = mine[half : half + 8]
    x_in[pl.ds(xi, 1)] = x_out[pl.ds(xi, 1)]
    stage(
        [
            exchange(x_out.at[p], x_in.at[xi], at_plane(yi, p, core), base + d)
            for d, p in enumerate(x_peers)
        ]
    )
    base += nx - 1
    mine = x_in[0]
    for j in range(1, nx):
        mine = mine + x_in[j]
    for j in range(ny):
        y_out[j, 0:piece, :] = mine[piece * j : piece * (j + 1)]
        y_out[j, piece : piece + 8, :] = mine[third : third + 8]
    y_in[pl.ds(yi, 1)] = y_out[pl.ds(yi, 1)]
    stage(
        [
            exchange(y_out.at[p], y_in.at[yi], at_plane(p, xi, core), base + d)
            for d, p in enumerate(y_peers)
        ]
    )
    base += ny - 1
    mine = y_in[0]
    for j in range(1, ny):
        mine = mine + y_in[j]
    mine = mine * norm
    gt_ref[...] = mine[piece : piece + 4]
    g2[pl.ds(yi, 1)] = mine[0:piece].reshape(1, piece, TB)
    stage(
        [
            exchange(g2.at[yi], g2.at[yi], at_plane(p, xi, core), base + d)
            for d, p in enumerate(y_peers)
        ]
    )
    base += ny - 1
    g1[pl.ds(xi, 1)] = g2[...].reshape(1, third, TB)
    stage(
        [
            exchange(g1.at[xi], g1.at[xi], at_plane(yi, p, core), base + d)
            for d, p in enumerate(x_peers)
        ]
    )
    base += nx - 1
    g0[pl.ds(core, 1)] = g1[...].reshape(1, half, TB)
    stage([exchange(g0.at[core], g0.at[core], partner, base)])
    whole = g0[...].reshape(512, TB)
    for d in range(2):
        gr_ref[d, 0] = whole[128 * d : 128 * d + 128]
        gm_ref[d, 0] = whole[256 + 128 * d : 384 + 128 * d]

    own_out.wait()
    wait_for_blocks(o_recv, n - 1)
    for _ in range(3):
        wait_for_blocks(z_send, n - 1)
    for copy in sent:
        copy.wait_send()


def store(*refs):
    count = len(refs) // 2
    sems = refs[-1]
    copies = [
        pltpu.make_async_copy(refs[j], refs[count + j], sems.at[j]) for j in range(count)
    ]
    for copy in copies:
        copy.start()
    for copy in copies:
        copy.wait()


def body(sizes, x, cotangent, taps, rate_map, gate_map, logit, spike):
    n, ny, nx, nc, _ = sizes
    length = n * TB
    half, third, piece = 512 // nc, 512 // nc // nx, 512 // nc // nx // ny
    messages = 2 * (nc + nx + ny - 3)
    vmem, hbm = pl.BlockSpec(memory_space=pltpu.VMEM), pl.BlockSpec(memory_space=pl.ANY)
    results = pl.pallas_call(
        functools.partial(kernel, sizes),
        name="recurrence_backward",
        out_shape=(
            pltpu.VMEM(x.shape, BF16),
            pltpu.VMEM(rate_map.shape, F32),
            pltpu.VMEM(gate_map.shape, F32),
            pltpu.VMEM(taps.shape, F32),
        ),
        in_specs=[hbm] * 7,
        out_specs=(vmem,) * 4,
        scratch_shapes=[
            pltpu.VMEM(taps.shape, BF16),
            pltpu.VMEM(rate_map.shape, BF16),
            pltpu.VMEM(gate_map.shape, BF16),
            pltpu.VMEM(logit.shape, F32),
            pltpu.VMEM((n, TB), F32),
            pltpu.VMEM((length, TB), BF16),
            pltpu.VMEM((length, TB), BF16),
            pltpu.VMEM((length + 16, TB), F32),
            pltpu.VMEM((length, TB), BF16),
            pltpu.VMEM((TB, length), BF16),
            pltpu.VMEM((TB, 512), BF16),
            pltpu.VMEM((length, 512), F32),
            pltpu.VMEM((2, length + 16, TB), F32),
            pltpu.VMEM((2, length, TB), F32),
            pltpu.VMEM((2, length, TB), F32),
            pltpu.VMEM((2, length, TB), F32),
            pltpu.VMEM((2, length, TB), F32),
            pltpu.VMEM((2, length, TB), F32),
            pltpu.VMEM((2, 4, length, TB), F32),
            pltpu.VMEM((2, length, TB), F32),
            pltpu.VMEM((2, 2, 8 * n, TB), F32),
            pltpu.VMEM((2, 8 * n, TB), F32),
            pltpu.VMEM((2, length, TB), F32),
            pltpu.VMEM((length + 32, TB), F32),
            pltpu.VMEM((max(1, n // 4) * TB + 32, TB), F32),
            pltpu.VMEM((length + 32, 512), BF16),
            pltpu.VMEM((length, TB), BF16),
            pltpu.VMEM((nc, half + 8, TB), F32),
            pltpu.VMEM((half + 8, TB), F32),
            pltpu.VMEM((nx, third + 8, TB), F32),
            pltpu.VMEM((nx, third + 8, TB), F32),
            pltpu.VMEM((ny, piece + 8, TB), F32),
            pltpu.VMEM((ny, piece + 8, TB), F32),
            pltpu.VMEM((ny, piece, TB), F32),
            pltpu.VMEM((nx, third, TB), F32),
            pltpu.VMEM((nc, half, TB), F32),
            pltpu.SemaphoreType.DMA((3,)),
            pltpu.SemaphoreType.DMA((5,)),
            pltpu.SemaphoreType.DMA,
            pltpu.SemaphoreType.DMA,
            pltpu.SemaphoreType.DMA((n - 1,)),
            pltpu.SemaphoreType.DMA,
            pltpu.SemaphoreType.DMA((messages,)),
            pltpu.SemaphoreType.DMA((messages,)),
        ],
        compiler_params=pltpu.CompilerParams(
            collective_id=0, has_side_effects=True, vmem_limit_bytes=56 * 1024 * 1024
        ),
    )(x, cotangent, taps, rate_map, gate_map, logit, spike.reshape(n, TB))
    return pl.pallas_call(
        store,
        name="store_results",
        out_shape=tuple(jax.ShapeDtypeStruct(r.shape, r.dtype) for r in results),
        in_specs=[vmem] * 4,
        out_specs=(hbm,) * 4,
        scratch_shapes=[pltpu.SemaphoreType.DMA((4,))],
    )(*[pltpu.with_memory_space_constraint(r, pltpu.VMEM) for r in results])


def solution(mesh):
    n, dp = mesh.shape["sp"], mesh.shape["dp"]
    ny, nx, nc = grid_of(dp)
    sizes = (n, ny, nx, nc, 1.0 / math.sqrt(dp * n * TB))
    return jax.shard_map(
        functools.partial(body, sizes),
        mesh=mesh,
        in_specs=(
            P("dp", "sp", None),
            P("dp", "sp", None),
            P(None, "sp"),
            P(None, "sp", None, None),
            P(None, "sp", None, None),
            P(None, "sp"),
            P("dp", "sp", None),
        ),
        out_specs=(
            P("dp", "sp", None),
            P(None, "sp", None, None),
            P(None, "sp", None, None),
            P(None, "sp"),
        ),
        check_vma=False,
    )
```

profile of v0, /device:TPU:1, one launch (start us, length us, event | category | flops | bytes accessed | tf_op | source)
XLA Modules:
  0.0 96.5 jit_solution(16643891237895369830)
XLA Ops:
  0.6 95.0 %recurrence_backward.1 = (bf16[1,128,2048]{2,1,0:T(8,128)(2,1)S(1)}, f32[2,1,128,128]{3,2,1,0:T(8,128)S(1)}, f32[2,1,128,128]{3,2,1,0:T(8,128)S(1)}, f32[4,128]{1,0:T(4,128)S(1)}) custom-call(bf16[1,128,2048]{2,1,0:T(8,128)(2,1)} %x_hbm.1, bf16[1,128,2048]{2,1,0:T(8,128)(2,1)} %cot_hbm.1, bf16[4,128]{1,0:T(4,128)(2,1)} %taps_hbm.1, ...), custom_call_target="tpu_custom_call" | custom-call | tf_op jit(solution)/shard_map/recurrence_backward/pallas_call | solution.py:525
  95.6 0.9 store_results.1
where the time goes:
time: 96.7 us; the launch traced here: 96.5 us
  Pallas kernels  95.9 us (99%)
    pallas_call x1, Pallas kernels, body(): pl.pallas_call(functools.partial(kernel, sizes), name='recurrence_backwar...  95 us

commit v1 on v0

--- a/solution.py
+++ b/solution.py
@@ -77,12 +77,15 @@
     wi_ref,
     logit_ref,
     spike_ref,
+    xs,
+    cs,
     xr,
     cr,
     xf,
     vs,
     vt,
     wcat,
+    wt,
     pre,
     af,
     sc,
@@ -116,6 +119,7 @@
     o_recv,
     r_send,
     r_recv,
+    joined,
 ):
     n, ny, nx, nc, norm = sizes
     length = n * TB
@@ -139,12 +143,17 @@
     partner = at_plane(yi, xi, 1 - core)
 
     barrier = pltpu.get_barrier_semaphore()
-    greet = [along_z(lax.rem(me + d, n)) for d in offsets]
-    greet += [at_plane(yi, x, core) for x in x_peers]
-    greet += [at_plane(y, xi, core) for y in y_peers]
-    greet += [partner]
-    for device in greet:
+    column = [along_z(lax.rem(me + d, n)) for d in offsets]
+    plane = [at_plane(yi, x, core) for x in x_peers]
+    plane += [at_plane(y, xi, core) for y in y_peers]
+    plane += [partner]
+    for device in column:
         pl.semaphore_signal(barrier, inc=1, device_id=device, device_id_type=MESH)
+
+    @pl.when(me == 0)
+    def _():
+        for device in plane:
+            pl.semaphore_signal(barrier, inc=1, device_id=device, device_id_type=MESH)
 
     def columns(ref, block):
         return ref.at[0, :, pl.ds(pl.multiple_of(block * TB, TB), TB)]
@@ -153,8 +162,8 @@
         return ref.at[pl.ds(pl.multiple_of(block * TB, TB), TB)]
 
     own = [
-        pltpu.make_async_copy(columns(x_hbm, me), rows_of(xr, me), local_sem.at[0]),
-        pltpu.make_async_copy(columns(cot_hbm, me), rows_of(cr, me), local_sem.at[1]),
+        pltpu.make_async_copy(x_hbm.at[0], xs, local_sem.at[0]),
+        pltpu.make_async_copy(cot_hbm.at[0], cs, local_sem.at[1]),
     ]
     own[0].start()
     own[1].start()
@@ -172,33 +181,43 @@
     ]
     for copy in small:
         copy.start()
-    pl.semaphore_wait(barrier, len(greet))
+
+    @pl.when(me > 0)
+    def _():
+        pl.semaphore_wait(barrier, len(column))
+
+    @pl.when(me == 0)
+    def _():
+        pl.semaphore_wait(barrier, len(column) + len(plane))
+
 
     def inward(which, k):
-        source, target = ((x_hbm, xr), (cot_hbm, cr))[which]
+        source, target = ((xs, xr), (cs, cr))[which]
         peer = lax.rem(me + offsets[k], n)
         return pltpu.make_async_remote_copy(
-            src_ref=columns(source, peer),
+            src_ref=source.at[:, pl.ds(pl.multiple_of(peer * TB, TB), TB)],
             dst_ref=rows_of(target, me),
             send_sem=z_send,
-            recv_sem=x_recv if which == 0 else c_recv.at[k],
+            recv_sem=x_recv if which == 0 else c_recv.at[(k + 1) // 2],
             device_id=along_z(peer),
             device_id_type=MESH,
         )
 
-    def cotangent_arrived(k):
-        near = n // 2 - (k + 1) // 2
-        origin = lax.rem(me + n - ((k % 2) * near + (1 - k % 2) * (n - near)), n)
-        pltpu.make_async_copy(rows_of(cr, origin), rows_of(cr, origin), c_recv.at[k]).wait()
-        return origin
+    def pair(j):
+        near = n // 2 - j
+        later = (j + n // 2 - 1) // (n // 2)
+        return lax.rem(me + near, n), lax.rem(me + n - near * later, n)
 
     def wait_for_blocks(sem, count):
         rows = pl.ds(0, count * TB)
         pltpu.make_async_copy(xr.at[rows], xr.at[rows], sem).wait()
 
-    for which in range(2):
+    mine = pl.ds(pl.multiple_of(me * TB, TB), TB)
+    for which, (source, target) in enumerate(((xs, xr), (cs, cr))):
+        own[which].wait()
         for k in range(n - 1):
             inward(which, k).start()
+        target[mine, :] = source[:, mine]
 
     for copy in small:
         copy.wait()
@@ -213,13 +232,21 @@
         af[d, length + 8 : length + 16, :] = zero_rows
         wcat[:, 256 * d : 256 * d + 128] = wr_ref[d, 0]
         wcat[:, 256 * d + 128 : 256 * d + 256] = wi_ref[d, 0]
+        for j, ref in enumerate((wr_ref, wi_ref)):
+            flipped = jnp.transpose(ref[d, 0].astype(F32)).astype(BF16)
+            wt[256 * d + 128 * j : 256 * d + 128 * j + 128, :] = flipped
     taps = [taps_ref[k : k + 1, :].astype(F32) for k in range(4)]
     keep = [STRENGTH * log_keep_of(logit_ref[d : d + 1, :]) for d in range(2)]
     row = lax.broadcasted_iota(jnp.int32, (8, 8, TB), 1)
     row0 = lax.broadcasted_iota(jnp.int32, (8, TB), 0)
 
-    own[0].wait()
     wait_for_blocks(x_recv, n - 1)
+
+    @pl.when(me == 0)
+    def _():
+        for device in plane:
+            pl.semaphore_signal(joined.at[0], inc=1, device_id=device, device_id_type=MESH)
+
 
     @pl.loop(0, n)
     def _(b):
@@ -326,15 +353,24 @@
                 carry = last_row(adjoint, forward)
         ends[d, 1, pl.ds(pl.multiple_of(block * 8, 8), 8), :] = carry
 
-    own[1].wait()
-    local_scan(0, me)
-    local_scan(1, me)
-
-    @pl.loop(0, n - 1)
-    def _(k):
-        origin = cotangent_arrived(k)
-        local_scan(0, origin)
-        local_scan(1, origin)
+    @pl.when(me == 0)
+    def _():
+        pl.semaphore_wait(joined.at[0], len(plane))
+        for device in column:
+            pl.semaphore_signal(joined.at[1], inc=1, device_id=device, device_id_type=MESH)
+
+    def scan_pair(j):
+        for block in pair(j):
+            local_scan(0, block)
+            local_scan(1, block)
+
+    wait_for_blocks(c_recv.at[0], 1)
+    scan_pair(0)
+
+    @pl.loop(1, n // 2)
+    def _(j):
+        wait_for_blocks(c_recv.at[j], 2)
+        scan_pair(j)
 
     ahead = back = start
     for b in range(n):
@@ -344,8 +380,7 @@
         carries[0, 8 * r : 8 * r + 8, :] = back
         back = ends[0, 1, 8 * r : 8 * r + 8, :] + ends[0, 0, 8 * r : 8 * r + 8, :] * back
 
-    @pl.loop(0, n)
-    def _(b):
+    def finish_block(b):
         incoming = [carries[d, pl.ds(pl.multiple_of(b * 8, 8), 8), :] for d in range(2)]
         for part in range(4):
             at = pl.multiple_of(b * TB + 32 * part, 32)
@@ -357,8 +392,8 @@
                 adjoint = (local + spread).reshape(32, TB)
                 bk[padded, 256 * d : 256 * d + 128] = (adjoint * e1[d, spot, :]).astype(BF16)
                 bk[padded, 256 * d + 128 : 256 * d + 256] = (adjoint * c2[d, spot, :]).astype(BF16)
-                piece_of = adjoint * c3[d, spot, :]
-                total = piece_of if total is None else total + piece_of
+                direct = adjoint * c3[d, spot, :]
+                total = direct if total is None else total + direct
             vd[padded, :] = total
 
     def outward(block):
@@ -371,33 +406,19 @@
             device_id_type=MESH,
         )
 
-    group = max(1, n // 4)
-    span = group * TB
-
-    def input_grad(step, sums):
-        turn = (1 - step // 2) * (2 + step) + (step // 2) * (3 - step)
-        part = lax.rem(me // group + turn, n // group)
-        base = pl.multiple_of(part * span, span)
-        vg[...] = vd[pl.ds(base, span + 32), :] + lax.dot_general(
-            bk[pl.ds(base, span + 32), :],
-            wcat[...],
-            (((1,), (1,)), ((), ())),
-            preferred_element_type=F32,
-        )
-        for inner in range(group):
-            block = part * group + inner
+    batch = min(4, n)
+
+    def input_grad(blocks, sums):
+        for i, block in enumerate(blocks):
+            wide = pl.ds(pl.multiple_of(block * TB, TB), TB + 32)
+            vg[i] = vd[wide, :] + jnp.dot(bk[wide, :], wt[...], preferred_element_type=F32)
+        for i, block in enumerate(blocks):
             at = pl.multiple_of(block * TB, TB)
-            low = 16 + inner * TB
-            here = vg[low : low + TB, :]
+            here = vg[i, 16 : 16 + TB, :]
             total = here * taps[2]
             for j in (0, 1, 3):
-                total = total + vg[low + 2 - j : low + 2 - j + TB, :] * taps[j]
+                total = total + vg[i, 18 - j : 18 - j + TB, :] * taps[j]
             go[pl.ds(at, TB), :] = total.astype(BF16)
-
-            @pl.when(block != me)
-            def _(block=block):
-                outward(block).start()
-
             sums = tuple(
                 sums[j]
                 + jnp.sum((xf[pl.ds(at + 6 + j, TB), :] * here).reshape(TB // 8, 8, TB), axis=0)
@@ -405,7 +426,21 @@
             )
         return sums
 
-    sums = lax.fori_loop(0, n // group, input_grad, (start,) * 4)
+    sums = (start,) * 4
+    finished = set()
+    for turn in (0, 1, 3, 2) if n // batch == 4 else range(n // batch):
+        first = n // 2 - batch // 2 + batch * turn
+        fresh = [r % n for r in range(first - 1, first + batch + 1)]
+        fresh = sorted(set(fresh) - finished)
+        finished.update(fresh)
+        for r in fresh:
+            finish_block(lax.rem(me + r, n))
+        apart = [r % n for r in range(first, first + batch)]
+        sums = input_grad([lax.rem(me + r, n) for r in apart], sums)
+        for r in sorted(apart, key=lambda r: -min(r, n - r)):
+            if r:
+                outward(lax.rem(me + r, n)).start()
+
     own_out = pltpu.make_async_copy(rows_of(go, me), columns(gi_ref, me), local_sem.at[2])
     own_out.start()
 
@@ -415,9 +450,10 @@
     piece = third // ny
     tap_rows = [jnp.sum(s, axis=0, keepdims=True) for s in sums]
     tile = jnp.concatenate(tap_rows + [jnp.zeros((4, TB), F32)], axis=0)
-    ordered = jnp.concatenate([maps[:, 128 * j : 128 * j + 128] for j in (0, 2, 1, 3)], axis=0)
+    for j, column in enumerate((0, 2, 1, 3)):
+        c, low = 128 * j // half, 128 * j % half
+        halves[c, low : low + 128, :] = maps[:, 128 * column : 128 * column + 128]
     for c in range(nc):
-        halves[c, 0:half, :] = ordered[half * c : half * (c + 1)]
         halves[c, half : half + 8, :] = tile
 
     def exchange(source, target, device, k):
@@ -432,28 +468,33 @@
 
     sent = []
 
-    def stage(copies):
+    @pl.when(me > 0)
+    def _():
+        pl.semaphore_wait(joined.at[1], 1)
+
+    def stage(copies, landing):
+        if not copies:
+            return
         for copy in copies:
             copy.start()
-        sent.extend(copies)
-        for copy in copies:
-            copy.wait_recv()
-
-    base = 0
-    stage([exchange(halves.at[1 - core], core_in, partner, base)])
-    base += 1
-    mine = halves[pl.ds(core, 1)][0] + core_in[...]
+        k = len(sent)
+        whole = landing.at[pl.ds(0, len(copies))]
+        sent.append(pltpu.make_async_copy(whole, whole, r_send.at[k]))
+        pltpu.make_async_copy(whole, whole, r_recv.at[k]).wait()
+
+    stage([exchange(halves.at[1 - core], core_in.at[0], partner, len(sent))], core_in)
+    mine = halves[pl.ds(core, 1)][0] + core_in[0]
     for j in range(nx):
         x_out[j, 0:third, :] = mine[third * j : third * (j + 1)]
         x_out[j, third : third + 8, :] = mine[half : half + 8]
     x_in[pl.ds(xi, 1)] = x_out[pl.ds(xi, 1)]
     stage(
         [
-            exchange(x_out.at[p], x_in.at[xi], at_plane(yi, p, core), base + d)
-            for d, p in enumerate(x_peers)
-        ]
+            exchange(x_out.at[p], x_in.at[xi], at_plane(yi, p, core), len(sent))
+            for p in x_peers
+        ],
+        x_in,
     )
-    base += nx - 1
     mine = x_in[0]
     for j in range(1, nx):
         mine = mine + x_in[j]
@@ -463,11 +504,11 @@
     y_in[pl.ds(yi, 1)] = y_out[pl.ds(yi, 1)]
     stage(
         [
-            exchange(y_out.at[p], y_in.at[yi], at_plane(p, xi, core), base + d)
-            for d, p in enumerate(y_peers)
-        ]
+            exchange(y_out.at[p], y_in.at[yi], at_plane(p, xi, core), len(sent))
+            for p in y_peers
+        ],
+        y_in,
     )
-    base += ny - 1
     mine = y_in[0]
     for j in range(1, ny):
         mine = mine + y_in[j]
@@ -476,21 +517,21 @@
     g2[pl.ds(yi, 1)] = mine[0:piece].reshape(1, piece, TB)
     stage(
         [
-            exchange(g2.at[yi], g2.at[yi], at_plane(p, xi, core), base + d)
-            for d, p in enumerate(y_peers)
-        ]
+            exchange(g2.at[yi], g2.at[yi], at_plane(p, xi, core), len(sent))
+            for p in y_peers
+        ],
+        g2,
     )
-    base += ny - 1
     g1[pl.ds(xi, 1)] = g2[...].reshape(1, third, TB)
     stage(
         [
-            exchange(g1.at[xi], g1.at[xi], at_plane(yi, p, core), base + d)
-            for d, p in enumerate(x_peers)
-        ]
+            exchange(g1.at[xi], g1.at[xi], at_plane(yi, p, core), len(sent))
+            for p in x_peers
+        ],
+        g1,
     )
-    base += nx - 1
     g0[pl.ds(core, 1)] = g1[...].reshape(1, half, TB)
-    stage([exchange(g0.at[core], g0.at[core], partner, base)])
+    stage([exchange(g0.at[core], g0.at[core], partner, len(sent))], g0)
     whole = g0[...].reshape(512, TB)
     for d in range(2):
         gr_ref[d, 0] = whole[128 * d : 128 * d + 128]
@@ -501,7 +542,7 @@
     for _ in range(3):
         wait_for_blocks(z_send, n - 1)
     for copy in sent:
-        copy.wait_send()
+        copy.wait()
 
 
 def store(*refs):
@@ -520,7 +561,6 @@
     n, ny, nx, nc, _ = sizes
     length = n * TB
     half, third, piece = 512 // nc, 512 // nc // nx, 512 // nc // nx // ny
-    messages = 2 * (nc + nx + ny - 3)
     vmem, hbm = pl.BlockSpec(memory_space=pltpu.VMEM), pl.BlockSpec(memory_space=pl.ANY)
     results = pl.pallas_call(
         functools.partial(kernel, sizes),
@@ -539,12 +579,15 @@
             pltpu.VMEM(gate_map.shape, BF16),
             pltpu.VMEM(logit.shape, F32),
             pltpu.VMEM((n, TB), F32),
+            pltpu.VMEM((TB, length), BF16),
+            pltpu.VMEM((TB, length), BF16),
             pltpu.VMEM((length, TB), BF16),
             pltpu.VMEM((length, TB), BF16),
             pltpu.VMEM((length + 16, TB), F32),
             pltpu.VMEM((length, TB), BF16),
             pltpu.VMEM((TB, length), BF16),
             pltpu.VMEM((TB, 512), BF16),
+            pltpu.VMEM((512, TB), BF16),
             pltpu.VMEM((length, 512), F32),
             pltpu.VMEM((2, length + 16, TB), F32),
             pltpu.VMEM((2, length, TB), F32),
@@ -558,11 +601,11 @@
             pltpu.VMEM((2, 8 * n, TB), F32),
             pltpu.VMEM((2, length, TB), F32),
             pltpu.VMEM((length + 32, TB), F32),
-            pltpu.VMEM((max(1, n // 4) * TB + 32, TB), F32),
+            pltpu.VMEM((min(4, n), TB + 32, TB), F32),
             pltpu.VMEM((length + 32, 512), BF16),
             pltpu.VMEM((length, TB), BF16),
             pltpu.VMEM((nc, half + 8, TB), F32),
-            pltpu.VMEM((half + 8, TB), F32),
+            pltpu.VMEM((1, half + 8, TB), F32),
             pltpu.VMEM((nx, third + 8, TB), F32),
             pltpu.VMEM((nx, third + 8, TB), F32),
             pltpu.VMEM((ny, piece + 8, TB), F32),
@@ -574,10 +617,11 @@
             pltpu.SemaphoreType.DMA((5,)),
             pltpu.SemaphoreType.DMA,
             pltpu.SemaphoreType.DMA,
-            pltpu.SemaphoreType.DMA((n - 1,)),
+            pltpu.SemaphoreType.DMA((n // 2,)),
             pltpu.SemaphoreType.DMA,
-            pltpu.SemaphoreType.DMA((messages,)),
-            pltpu.SemaphoreType.DMA((messages,)),
+            pltpu.SemaphoreType.DMA((6,)),
+            pltpu.SemaphoreType.DMA((6,)),
+            pltpu.SemaphoreType.REGULAR((2,)),
         ],
         compiler_params=pltpu.CompilerParams(
             collective_id=0, has_side_effects=True, vmem_limit_bytes=56 * 1024 * 1024

time: 96.7 us -> 93.2 us (0.964)
  Pallas kernels: 95.9 us -> 92.4 us
    pallas_call x1, Pallas kernels: 95 us -> 91.5 us  [body(): pl.pallas_call(functools.partial(kernel, sizes), name='recurrence_backwar...]
where the time goes in v1:
time: 93.2 us; the launch traced here: 93.1 us
  Pallas kernels  92.4 us (99%)
    pallas_call x1, Pallas kernels, body(): pl.pallas_call(functools.partial(kernel, sizes), name='recurrence_backwar...  91.5 us

profile of v1, /device:TPU:1, one launch (start us, length us, event | category | flops | bytes accessed | tf_op | source)
XLA Modules:
  0.0 93.1 jit_solution(13443550178771576873)
XLA Ops:
  0.6 91.5 %recurrence_backward.1 = (bf16[1,128,2048]{2,1,0:T(8,128)(2,1)S(1)}, f32[2,1,128,128]{3,2,1,0:T(8,128)S(1)}, f32[2,1,128,128]{3,2,1,0:T(8,128)S(1)}, f32[4,128]{1,0:T(4,128)S(1)}) custom-call(bf16[1,128,2048]{2,1,0:T(8,128)(2,1)} %x_hbm.1, bf16[1,128,2048]{2,1,0:T(8,128)(2,1)} %cot_hbm.1, bf16[4,128]{1,0:T(4,128)(2,1)} %taps_hbm.1, ...), custom_call_target="tpu_custom_call" | custom-call | tf_op jit(solution)/shard_map/recurrence_backward/pallas_call | solution.py:565
  92.1 0.9 store_results.1

commit v2 on v1

--- a/solution.py
+++ b/solution.py
@@ -408,7 +408,7 @@
 
     batch = min(4, n)
 
-    def input_grad(blocks, sums):
+    def input_grad(blocks, away, sums):
         for i, block in enumerate(blocks):
             wide = pl.ds(pl.multiple_of(block * TB, TB), TB + 32)
             vg[i] = vd[wide, :] + jnp.dot(bk[wide, :], wt[...], preferred_element_type=F32)
@@ -419,6 +419,8 @@
             for j in (0, 1, 3):
                 total = total + vg[i, 18 - j : 18 - j + TB, :] * taps[j]
             go[pl.ds(at, TB), :] = total.astype(BF16)
+            if away[i]:
+                outward(block).start()
             sums = tuple(
                 sums[j]
                 + jnp.sum((xf[pl.ds(at + 6 + j, TB), :] * here).reshape(TB // 8, 8, TB), axis=0)
@@ -436,10 +438,8 @@
         for r in fresh:
             finish_block(lax.rem(me + r, n))
         apart = [r % n for r in range(first, first + batch)]
-        sums = input_grad([lax.rem(me + r, n) for r in apart], sums)
-        for r in sorted(apart, key=lambda r: -min(r, n - r)):
-            if r:
-                outward(lax.rem(me + r, n)).start()
+        apart = sorted(apart, key=lambda r: -min(r, n - r))
+        sums = input_grad([lax.rem(me + r, n) for r in apart], apart, sums)
 
     own_out = pltpu.make_async_copy(rows_of(go, me), columns(gi_ref, me), local_sem.at[2])
     own_out.start()

time: 93.2 us -> 93.3 us (level)
  no operation moved by 1% of the time
where the time goes in v2:
time: 93.3 us; the launch traced here: 93.2 us
  Pallas kernels  92.5 us (99%)
    pallas_call x1, Pallas kernels, body(): pl.pallas_call(functools.partial(kernel, sizes), name='recurrence_backwar...  91.6 us

profile of v2, /device:TPU:1, one launch (start us, length us, event | category | flops | bytes accessed | tf_op | source)
XLA Modules:
  0.0 93.2 jit_solution(15071033951175897397)
XLA Ops:
  0.6 91.6 %recurrence_backward.1 = (bf16[1,128,2048]{2,1,0:T(8,128)(2,1)S(1)}, f32[2,1,128,128]{3,2,1,0:T(8,128)S(1)}, f32[2,1,128,128]{3,2,1,0:T(8,128)S(1)}, f32[4,128]{1,0:T(4,128)S(1)}) custom-call(bf16[1,128,2048]{2,1,0:T(8,128)(2,1)} %x_hbm.1, bf16[1,128,2048]{2,1,0:T(8,128)(2,1)} %cot_hbm.1, bf16[4,128]{1,0:T(4,128)(2,1)} %taps_hbm.1, ...), custom_call_target="tpu_custom_call" | custom-call | tf_op jit(solution)/shard_map/recurrence_backward/pallas_call | solution.py:565
  92.3 0.9 store_results.1
